TPU v7x, 256 devices: a 4x2x16 block of a 4x16x16 slice. The times are simulated.
256 devices in a mesh: grp: 2 (over y), fs: 32 (over z, core), tp: 4 (over x).
Axes of the slice: x: 4, y: 2, z: 16, core: 2. Of those that a mesh axis runs over, the one named last changes fastest.
The devices are a block of a 4x16x16 slice.
Arguments:
- tokens: bfloat16 [1536, 2048], P(('grp', 'tp')), parts along dimension 0, may hold values from -6 to 6
- norm_gain: float32 [2048], P('fs'), may hold values from 0.1 to 1.9
- up_trained: float32 [2048, 8192], P('fs', 'tp'), may hold values from -0.125 to 0.125
- down_trained: float32 [2048, 8192], P('fs', 'tp'), may hold values from -0.125 to 0.125
Outputs:
- up_serving: bfloat16 [4096, 8192], P('grp', 'fs'), parts along dimension 0
- down_serving: bfloat16 [4096, 8192], P('grp', 'fs'), parts along dimension 0
- prompt_output: bfloat16 [1536, 2048], P(('grp', 'tp'), 'fs'), parts along dimension 0
There are 2 independent parts, one for each index of `grp`. A program takes and returns all parts, laid end to end along the dimension named above; an argument that names none is the same for every part. Nothing has to cross between parts.
All inputs are finite; a program needn't handle non-finite values.
Results may differ from a plain program's by a relative error of at most 0.0074.
Values may be sent and summed in bfloat16 or wider, within the bound.
No kernel may reach another device: no remote copies, remote signals or barrier semaphores. Data moves between devices by JAX's collectives and lax.ppermute only.
A program may use at most 64 MiB of HBM per device.

v0:
```python
import jax
import jax.numpy as jnp
from jax import lax
from jax.sharding import PartitionSpec as P

epsilon = 1e-06


def joined_along(parts, dim):
    parts = jnp.moveaxis(parts, 0, dim)
    dims = parts.shape
    return parts.reshape(*dims[:dim], dims[dim] * dims[dim + 1], *dims[dim + 2 :])


def copy_for_each(x, axis):
    devices = lax.axis_size(axis)
    return lax.all_to_all(jnp.broadcast_to(x[None], (devices, *x.shape)), axis, 0, 0, tiled=True)


def collect(x, axis, dim):
    return joined_along(copy_for_each(x, axis), dim)


def in_blocks(x, dim, devices):
    dims = x.shape
    parts = x.reshape(*dims[:dim], devices, dims[dim] // devices, *dims[dim + 1 :])
    return jnp.moveaxis(parts, dim, 0)


def sum_at_owner(x, axis, dim):
    parts = in_blocks(x, dim, lax.axis_size(axis))
    arrived = lax.all_to_all(parts, axis, split_axis=0, concat_axis=0, tiled=True)
    return arrived.astype(jnp.float32).sum(axis=0)


def local(tokens, norm_gain, up_trained, down_trained):
    shards = lax.axis_size("fs")
    groups = lax.axis_size("tp")
    rows_local = up_trained.shape[0]
    cols_local = up_trained.shape[1]
    folded = (norm_gain[:, None] * up_trained).astype(jnp.bfloat16)
    stacked = jnp.stack([folded, down_trained.astype(jnp.bfloat16)])
    served_width = cols_local * groups // shards
    blocks_here = cols_local // served_width
    quarter_rows = rows_local // groups
    pieces = stacked.reshape(2, groups, quarter_rows, blocks_here, served_width)
    moved = lax.all_to_all(pieces, "tp", split_axis=1, concat_axis=3, tiled=True)
    placed = lax.all_to_all(moved, "fs", split_axis=3, concat_axis=2, tiled=True)
    ordered = placed.reshape(2, shards, quarter_rows, served_width)
    joined = collect(ordered, "tp", 2)
    owned = joined.reshape(2, rows_local * shards, served_width)
    up_serving = owned[0]
    down_serving = owned[1]
    values = tokens.astype(jnp.float32)
    scale = lax.rsqrt(jnp.mean(values * values, axis=1, keepdims=True) + epsilon)
    normed = (values * scale).astype(jnp.bfloat16)
    hidden = jnp.dot(normed, up_serving, preferred_element_type=jnp.float32)
    active = jnp.square(jax.nn.relu(hidden)).astype(jnp.bfloat16)
    summed = sum_at_owner(
        lax.dot_general(
            down_serving, active, (((1,), (1,)), ((), ())), preferred_element_type=jnp.float32
        ).astype(jnp.bfloat16),
        "fs",
        0,
    )
    prompt_output = summed.T.astype(jnp.bfloat16)
    return (up_serving, down_serving, prompt_output)


def solution(mesh):
    in_specs = (P(("grp", "tp"), None), P("fs"), P("fs", "tp"), P("fs", "tp"))
    out_specs = (P("grp", "fs"), P("grp", "fs"), P(("grp", "tp"), "fs"))
    return jax.shard_map(local, mesh=mesh, in_specs=in_specs, out_specs=out_specs, check_vma=False)
```

profile of v0, /device:TPU:40, one launch (start us, length us, event | category | flops | bytes accessed | tf_op | source)
XLA Modules:
  0.0 170.9 jit_solution(14890770866300171647)
XLA Ops:
  0.6 0.0 copy-start.3
  0.6 1.2 multiply_convert_fusion
  1.8 0.1 copy.23
  1.9 0.0 copy-done.3
  2.0 0.1 copy.24
  2.0 0.1 pad_maximum_fusion
  2.1 13.9 %all_to_all.43 = bf16[2,4,16,8,256]{4,3,2,0,1:T(8,128)(2,1)S(1)} all-to-all(bf16[2,4,16,8,256]{4,3,2,0,1:T(8,128)(2,1)S(1)} %copy.17), channel_id=1, replica_groups=mesh['grp'=2,'fs'=32,'tp'=4] {'tp'}, dimensions={1} | all-to-all | bytes 1048576 | tf_op jit(solution)/shard_map/all_to_all | solution.py:47
  16.0 0.1 copy.28
  16.1 0.3 copy.19
  16.4 57.6 %all_to_all.44 = bf16[2,1,16,32,256]{4,2,0,1,3:T(8,128)(2,1)S(1)} all-to-all(bf16[2,1,16,32,256]{4,2,0,1,3:T(8,128)(2,1)S(1)} %copy.19), channel_id=1, replica_groups=mesh['grp'=2,'fs'=32,'tp'=4] {'fs'}, dimensions={3} | all-to-all | bytes 1048576 | tf_op jit(solution)/shard_map/all_to_all | solution.py:48
  74.1 1.5 broadcast_in_dim.10
  75.6 3.8 %all-to-all-start.2 = ((bf16[4,2,32,16,256]{4,3,2,1,0:T(8,128)(2,1)}), bf16[4,2,32,16,256]{4,3,2,1,0:T(8,128)(2,1)S(1)}, u32[]{:S(2)}, u32[]{:S(2)}) async-start(bf16[4,2,32,16,256]{4,3,2,1,0:T(8,128)(2,1)} %broadcast_in_dim.10), calls=%async_computation.2 | async-start | bytes 4194304 | tf_op jit(solution)/shard_map/all_to_all | solution.py:17
  79.4 0.0 copy-done.2
  79.5 0.2 fusion
  79.7 26.4 %all-to-all-done.2 = bf16[4,2,32,16,256]{4,3,2,1,0:T(8,128)(2,1)S(1)} async-done(((bf16[4,2,32,16,256]{4,3,2,1,0:T(8,128)(2,1)}), bf16[4,2,32,16,256]{4,3,2,1,0:T(8,128)(2,1)S(1)}, u32[]{:S(2)}, u32[]{:S(2)}) %all-to-all-start.2) | async-done | bytes 2097184 | tf_op jit(solution)/shard_map/all_to_all | solution.py:17
  106.1 0.3 copy.27
  106.4 0.2 fusion.10
  106.7 0.0 copy-start.1
  106.7 0.0 copy-start
  106.7 0.9 copy-done.1
  107.7 2.3 %convolution_convert_fusion = bf16[2048,192]{0,1:T(8,128)(2,1)S(1)} fusion(bf16[2048,256]{1,0:T(8,128)(2,1)S(1)} %bitcast.29, bf16[2048,256]{1,0:T(8,128)(2,1)S(1)} %bitcast.31, bf16[192,2048]{1,0:T(8,128)(2,1)} %param.4, f32[192]{0:T(256)S(1)} %add_rsqrt_fusion), kind=kOutput, calls=%fused_computation | convolution fusion | flops 404373504 | bytes 3670784 | tf_op jit(solution)/shard_map/dot_general | solution.py:60
  110.0 0.5 copy.22
  110.5 59.6 %all_to_all.45 = bf16[32,64,192]{2,1,0:T(8,128)(2,1)S(1)} all-to-all(bf16[32,64,192]{2,1,0:T(8,128)(2,1)S(1)} %bitcast.28), channel_id=1, replica_groups=mesh['grp'=2,'fs'=32,'tp'=4] {'fs'}, dimensions={0} | all-to-all | bytes 1572864 | tf_op jit(solution)/shard_map/all_to_all | solution.py:32
  170.1 0.8 reduce_sum.22
  (6 shorter events, 0.1 us)
Async XLA Ops:
  0.6 1.3 copy-start.3
  75.6 3.8 %copy-start.2 = (bf16[192,2048]{1,0:T(8,128)(2,1)S(1)}, bf16[192,2048]{1,0:T(8,128)(2,1)}, u32[]{:S(2)}) copy-start(bf16[192,2048]{1,0:T(8,128)(2,1)} %param.4) | copy-start | bytes 2359300
  75.6 30.5 %all-to-all-start.2 = ((bf16[4,2,32,16,256]{4,3,2,1,0:T(8,128)(2,1)}), bf16[4,2,32,16,256]{4,3,2,1,0:T(8,128)(2,1)S(1)}, u32[]{:S(2)}, u32[]{:S(2)}) async-start(bf16[4,2,32,16,256]{4,3,2,1,0:T(8,128)(2,1)} %broadcast_in_dim.10), calls=%async_computation.2 | async-start | bytes 4194304 | tf_op jit(solution)/shard_map/all_to_all | solution.py:17
  106.7 1.0 copy-start.1
  106.7 3.3 %copy-start = (bf16[1,32,4,16,256]{4,3,2,1,0:T(8,128)(2,1)}, bf16[1,32,4,16,256]{4,3,2,1,0:T(8,128)(2,1)S(1)}, u32[]{:S(2)}) copy-start(bf16[1,32,4,16,256]{4,3,2,1,0:T(8,128)(2,1)S(1)} %get-tuple-element.3) | copy-start | bytes 3145732
where the time goes:
time: 172 us; the launch traced here: 171 us
  blocking collectives  131 us (76%)
  waiting for transfers between devices  26.4 us (15%)
  local copies, waits for them, and re-layouts  4.06 us (2%)
  starting transfers between devices  3.83 us (2%)
  other arithmetic  2.33 us (1%)
  matrix products  2.28 us (1%)
    all_to_all x1, blocking collectives, sum_at_owner(): lax.all_to_all(parts, axis, split_axis=0, concat_axis=0, tiled=True)  59.6 us
    all_to_all x1, blocking collectives, local(): lax.all_to_all(moved, 'fs', split_axis=3, concat_axis=2, tiled=True)  57.6 us
    all_to_all x1, waiting for transfers between devices, copy_for_each(): lax.all_to_all(jnp.broadcast_to(x[None], (devices, *x.shape)), axis, 0, 0...  26.4 us
    all_to_all x1, blocking collectives, local(): lax.all_to_all(pieces, 'tp', split_axis=1, concat_axis=3, tiled=True)  13.9 us
    all_to_all x1, starting transfers between devices, copy_for_each(): lax.all_to_all(jnp.broadcast_to(x[None], (devices, *x.shape)), axis, 0, 0...  3.83 us
  transfers between devices with their start and end apart: 1, of which 1 were waited for; matrix products, arithmetic and copies ran while one was open for 0% of the time, Pallas kernels for 0%

commit v1 on v0

--- a/solution.py
+++ b/solution.py
@@ -4,6 +4,7 @@
 from jax.sharding import PartitionSpec as P
 
 epsilon = 1e-06
+CORES = 2
 
 
 def joined_along(parts, dim):
@@ -21,16 +22,34 @@
     return joined_along(copy_for_each(x, axis), dim)
 
 
-def in_blocks(x, dim, devices):
-    dims = x.shape
-    parts = x.reshape(*dims[:dim], devices, dims[dim] // devices, *dims[dim + 1 :])
-    return jnp.moveaxis(parts, dim, 0)
+def packed(x):
+    rows, cols = x.shape[-2:]
+    wide = cols * 2 // 3
+    tail = x[..., wide:]
+    tail = jnp.concatenate([tail[..., : rows // 2, :], tail[..., rows // 2 :, :]], axis=-1)
+    return jnp.concatenate([x[..., :wide], tail], axis=-2)
 
 
-def sum_at_owner(x, axis, dim):
-    parts = in_blocks(x, dim, lax.axis_size(axis))
-    arrived = lax.all_to_all(parts, axis, split_axis=0, concat_axis=0, tiled=True)
-    return arrived.astype(jnp.float32).sum(axis=0)
+def unpacked(x, rows):
+    wide = x.shape[-1]
+    tail = x[..., rows:, :]
+    tail = jnp.concatenate([tail[..., : wide // 2], tail[..., wide // 2 :]], axis=-2)
+    return jnp.concatenate([x[..., :rows, :], tail], axis=-1)
+
+
+def sum_at_owner(x, axis):
+    devices = lax.axis_size(axis)
+    rows = x.shape[0] // devices
+    chips = devices // CORES
+    parts = packed(x.reshape(chips, CORES, rows, x.shape[1]))
+    core = lax.axis_index(axis) % CORES
+    away = lax.dynamic_index_in_dim(parts, 1 - core, 1, keepdims=False)
+    kept = lax.dynamic_index_in_dim(parts, core, 1, keepdims=False)
+    other = lax.ppermute(away, axis, [(i, i ^ 1) for i in range(devices)])
+    both = (kept.astype(jnp.float32) + other.astype(jnp.float32)).astype(jnp.bfloat16)
+    same_core = [[z * CORES + c for z in range(chips)] for c in range(CORES)]
+    arrived = lax.all_to_all(both, axis, 0, 0, axis_index_groups=same_core, tiled=True)
+    return unpacked(arrived.astype(jnp.float32).sum(axis=0), rows)
 
 
 def local(tokens, norm_gain, up_trained, down_trained):
@@ -56,14 +75,10 @@
     normed = (values * scale).astype(jnp.bfloat16)
     hidden = jnp.dot(normed, up_serving, preferred_element_type=jnp.float32)
     active = jnp.square(jax.nn.relu(hidden)).astype(jnp.bfloat16)
-    summed = sum_at_owner(
-        lax.dot_general(
-            down_serving, active, (((1,), (1,)), ((), ())), preferred_element_type=jnp.float32
-        ).astype(jnp.bfloat16),
-        "fs",
-        0,
-    )
-    prompt_output = summed.T.astype(jnp.bfloat16)
+    partial = lax.dot_general(
+        down_serving, active, (((1,), (1,)), ((), ())), preferred_element_type=jnp.float32
+    ).astype(jnp.bfloat16)
+    prompt_output = sum_at_owner(partial, "fs").T.astype(jnp.bfloat16)
     return (up_serving, down_serving, prompt_output)
 
 

time: 172 us -> 142 us (0.83)
  blocking collectives: 131 us -> 99.1 us
    all_to_all x1, blocking collectives: 59.6 us -> 27.5 us  [sum_at_owner(): lax.all_to_all(both, axis, 0, 0, axis_index_groups=same_core, tiled=True)]
  transfers between devices with their start and end apart: 1 -> 2, of which waited for: 1 -> 2; matrix products, arithmetic and copies ran while one was open for 0% -> 0% of each run, Pallas kernels for 0% -> 0%
where the time goes in v1:
time: 142 us
  blocking collectives  99.1 us (70%)
  waiting for transfers between devices  28.1 us (20%)
  local copies, waits for them, and re-layouts  4.34 us (3%)
  starting transfers between devices  3.97 us (3%)
  other arithmetic  3.16 us (2%)
  matrix products  2.05 us (1%)
    all_to_all x1, blocking collectives, local(): lax.all_to_all(moved, 'fs', split_axis=3, concat_axis=2, tiled=True)  57.6 us
    all_to_all x1, blocking collectives, sum_at_owner(): lax.all_to_all(both, axis, 0, 0, axis_index_groups=same_core, tiled=True)  27.5 us
    all_to_all x1, waiting for transfers between devices, copy_for_each(): lax.all_to_all(jnp.broadcast_to(x[None], (devices, *x.shape)), axis, 0, 0...  26.4 us
    all_to_all x1, blocking collectives, local(): lax.all_to_all(pieces, 'tp', split_axis=1, concat_axis=3, tiled=True)  13.9 us
    all_to_all x1, starting transfers between devices, copy_for_each(): lax.all_to_all(jnp.broadcast_to(x[None], (devices, *x.shape)), axis, 0, 0...  3.83 us
  transfers between devices with their start and end apart: 2, of which 2 were waited for; matrix products, arithmetic and copies ran while one was open for 0% of the time, Pallas kernels for 0%

profile of v1, /device:TPU:40, one launch (start us, length us, event | category | flops | bytes accessed | tf_op | source)
XLA Modules:
  0.0 141.5 jit_solution(10750599824275625618)
XLA Ops:
  0.6 1.1 convert_element_type.38
  1.8 0.8 multiply_convert_fusion
  2.8 13.9 %all_to_all.43 = bf16[2,4,16,8,256]{4,3,2,0,1:T(8,128)(2,1)S(1)} all-to-all(bf16[2,4,16,8,256]{4,3,2,0,1:T(8,128)(2,1)S(1)} %copy.17), channel_id=1, replica_groups=mesh['grp'=2,'fs'=32,'tp'=4] {'tp'}, dimensions={1} | all-to-all | bytes 1048576 | tf_op jit(solution)/shard_map/all_to_all | solution.py:66
  16.7 0.1 copy.28
  16.8 0.3 copy.19
  17.1 57.6 %all_to_all.44 = bf16[2,1,16,32,256]{4,2,0,1,3:T(8,128)(2,1)S(1)} all-to-all(bf16[2,1,16,32,256]{4,2,0,1,3:T(8,128)(2,1)S(1)} %copy.19), channel_id=1, replica_groups=mesh['grp'=2,'fs'=32,'tp'=4] {'fs'}, dimensions={3} | all-to-all | bytes 1048576 | tf_op jit(solution)/shard_map/all_to_all | solution.py:67
  74.7 1.5 %broadcast_in_dim.10 = bf16[4,2,32,16,256]{4,3,2,1,0:T(8,128)(2,1)} broadcast(bf16[2,32,16,256]{3,2,1,0:T(8,128)(2,1)S(1)} %copy.20), dimensions={1,2,3,4} | broadcast | bytes 2621440 | tf_op jit(solution)/shard_map/broadcast_in_dim | solution.py:18
  76.2 3.8 %all-to-all-start.2 = ((bf16[4,2,32,16,256]{4,3,2,1,0:T(8,128)(2,1)}), bf16[4,2,32,16,256]{4,3,2,1,0:T(8,128)(2,1)S(1)}, u32[]{:S(2)}, u32[]{:S(2)}) async-start(bf16[4,2,32,16,256]{4,3,2,1,0:T(8,128)(2,1)} %broadcast_in_dim.10), calls=%async_computation.2 | async-start | bytes 4194304 | tf_op jit(solution)/shard_map/all_to_all | solution.py:18
  80.1 0.2 fusion
  80.4 26.4 %all-to-all-done.2 = bf16[4,2,32,16,256]{4,3,2,1,0:T(8,128)(2,1)S(1)} async-done(((bf16[4,2,32,16,256]{4,3,2,1,0:T(8,128)(2,1)}), bf16[4,2,32,16,256]{4,3,2,1,0:T(8,128)(2,1)S(1)}, u32[]{:S(2)}, u32[]{:S(2)}) %all-to-all-start.2) | async-done | bytes 2097184 | tf_op jit(solution)/shard_map/all_to_all | solution.py:18
  106.8 0.3 copy.27
  107.1 0.2 fusion.11
  107.3 2.0 %convolution_convert_fusion = bf16[2048,192]{0,1:T(8,128)(2,1)} fusion(bf16[2048,256]{1,0:T(8,128)(2,1)S(1)} %bitcast.36, bf16[2048,256]{1,0:T(8,128)(2,1)S(1)} %bitcast.38, bf16[192,2048]{1,0:T(8,128)(2,1)S(1)} %copy-done.2, f32[192]{0:T(256)S(1)} %add_rsqrt_fusion), kind=kOutput, calls=%fused_computation | convolution fusion | flops 404373504 | bytes 3670784 | tf_op jit(solution)/shard_map/dot_general | solution.py:78
  109.4 1.4 %copy.22 = bf16[2048,192]{1,0:T(8,128)(2,1)S(1)} copy(bf16[2048,192]{0,1:T(8,128)(2,1)} %convolution_convert_fusion) | data formatting | bytes 1572864 | tf_op jit(solution)/shard_map/convert_element_type | solution.py:80
  110.8 0.1 fusion.12
  110.9 0.1 slice.45
  111.1 0.2 maximum_maximum_fusion
  111.3 0.1 collective-permute-start
  111.5 1.7 %collective-permute-done = bf16[16,96,128]{2,1,0:T(8,128)(2,1)S(1)} collective-permute-done((bf16[16,96,128]{2,1,0:T(8,128)(2,1)S(1)}, bf16[16,96,128]{2,1,0:T(8,128)(2,1)S(1)}, u32[]{:S(2)}, u32[]{:S(2)}) %collective-permute-start) | collective-permute-done | bytes 393248 | tf_op jit(solution)/shard_map/ppermute | solution.py:48
  113.1 0.1 fusion.6
  113.3 27.5 %all_to_all.45 = bf16[16,96,128]{2,1,0:T(8,128)(2,1)S(1)} all-to-all(bf16[16,96,128]{2,1,0:T(8,128)(2,1)S(1)} %fusion.6), channel_id=1, replica_groups={{0,8,16,24,32,40,48,56,64,72,80,88,96,104,112,120},{4,12,20,28,36,44,52..., dimensions={0} | all-to-all | bytes 786432 | tf_op jit(solution)/shard_map/all_to_all | solution.py:51
  140.8 0.1 reduce
  140.8 0.1 fusion.13
  140.9 0.6 maximum_bitcast_fusion
  (16 shorter events, 0.3 us)
Async XLA Ops:
  0.6 1.2 copy-start.3
  76.2 3.9 %copy-start.2 = (bf16[192,2048]{1,0:T(8,128)(2,1)S(1)}, bf16[192,2048]{1,0:T(8,128)(2,1)}, u32[]{:S(2)}) copy-start(bf16[192,2048]{1,0:T(8,128)(2,1)} %param.4) | copy-start | bytes 2359300
  76.2 30.5 %all-to-all-start.2 = ((bf16[4,2,32,16,256]{4,3,2,1,0:T(8,128)(2,1)}), bf16[4,2,32,16,256]{4,3,2,1,0:T(8,128)(2,1)S(1)}, u32[]{:S(2)}, u32[]{:S(2)}) async-start(bf16[4,2,32,16,256]{4,3,2,1,0:T(8,128)(2,1)} %broadcast_in_dim.10), calls=%async_computation.2 | async-start | bytes 4194304 | tf_op jit(solution)/shard_map/all_to_all | solution.py:18
  107.3 2.1 %copy-start = (bf16[1,32,4,16,256]{4,3,2,1,0:T(8,128)(2,1)}, bf16[1,32,4,16,256]{4,3,2,1,0:T(8,128)(2,1)S(1)}, u32[]{:S(2)}) copy-start(bf16[1,32,4,16,256]{4,3,2,1,0:T(8,128)(2,1)S(1)} %get-tuple-element.3) | copy-start | bytes 3145732
  107.3 2.1 %copy-start.1 = (bf16[1,32,4,16,256]{4,3,2,1,0:T(8,128)(2,1)}, bf16[1,32,4,16,256]{4,3,2,1,0:T(8,128)(2,1)S(1)}, u32[]{:S(2)}) copy-start(bf16[1,32,4,16,256]{4,3,2,1,0:T(8,128)(2,1)S(1)} %get-tuple-element.4) | copy-start | bytes 3145732
  111.3 1.8 %collective-permute-start = (bf16[16,96,128]{2,1,0:T(8,128)(2,1)S(1)}, bf16[16,96,128]{2,1,0:T(8,128)(2,1)S(1)}, u32[]{:S(2)}, u32[]{:S(2)}) collective-permute-start(bf16[16,96,128]{2,1,0:T(8,128)(2,1)S(1)} %dynamic-slice_bitcast_fusion), channel_id=1, source_target_pairs={{0,4},{4,0},{8,12},{12,8},{16,20},{20,16},{24,28},{28,24},{32,36},... | collective-permute-start | bytes 1179656 | tf_op jit(solution)/shard_map/ppermute | solution.py:48

commit v2 on v0

v2 whole, which is shorter than its diff:
```python
import functools

import jax
import jax.numpy as jnp
from jax import lax
from jax.experimental import pallas as pl
from jax.experimental.pallas import tpu as pltpu
from jax.sharding import PartitionSpec as P

epsilon = 1e-06
CORES = 2
LANES = 128


def ring(devices, step):
    return [(i, (i + step) % devices) for i in range(devices)]


def nt_dot(a, b):
    return lax.dot_general(a, b, (((1,), (1,)), ((), ())), preferred_element_type=jnp.float32)


def feed_forward(
    where, normed, own, left, right, far_up, far_down, up_out, down_out, kept, away, up, down, sems
):
    shards, groups, quarter, width = up.shape
    at, core = where[0], where[1]
    for step, (piece_up, piece_down) in enumerate(
        [(own.at[0], own.at[1]), (left.at[0], left.at[1]), (far_up, far_down), (right.at[0], right.at[1])]
    ):
        slot = lax.rem(at + step, groups)
        up[:, pl.ds(slot, 1)] = piece_up[...][:, None]
        down[:, pl.ds(slot, 1)] = piece_down[...][:, None]
    writes = [pltpu.make_async_copy(up, up_out, sems.at[0]), pltpu.make_async_copy(down, down_out, sems.at[1])]
    for write in writes:
        write.start()
    hidden = jnp.dot(
        normed[...], up[...].reshape(shards * groups * quarter, width), preferred_element_type=jnp.float32
    )
    active = jnp.square(jnp.maximum(hidden, 0.0)).astype(jnp.bfloat16)
    head, tail = active[:LANES], active[LANES:]
    none = jnp.zeros_like(tail)
    upper, lower = jnp.concatenate([tail, none]), jnp.concatenate([none, tail])
    rows, chips = groups * quarter, shards // CORES
    for out, side in ((away, 1 - core), (kept, core)):
        weights = down.reshape(chips, CORES, rows, width)[:, pl.ds(side, 1)][:, 0]
        out[:, :rows] = nt_dot(weights.reshape(chips * rows, width), head).astype(out.dtype).reshape(chips, rows, LANES)
        both = nt_dot(weights[:, : rows // 2].reshape(chips * rows // 2, width), upper) + nt_dot(
            weights[:, rows // 2 :].reshape(chips * rows // 2, width), lower
        )
        out[:, rows:] = both.astype(out.dtype).reshape(chips, rows // 2, LANES)
    for write in writes:
        write.wait()


def unpacked(x, rows):
    tail = x[rows:]
    tail = jnp.concatenate([tail[:, : LANES // 2], tail[:, LANES // 2 :]], axis=0)
    return jnp.concatenate([x[:rows], tail], axis=1)


def local(tokens, norm_gain, up_trained, down_trained):
    shards = lax.axis_size("fs")
    groups = lax.axis_size("tp")
    chips = shards // CORES
    rows_local, cols_local = up_trained.shape
    count, features = tokens.shape
    folded = (norm_gain[:, None] * up_trained).astype(jnp.bfloat16)
    stacked = jnp.stack([folded, down_trained.astype(jnp.bfloat16)])
    width = cols_local * groups // shards
    blocks_here = cols_local // width
    quarter = rows_local // groups
    pieces = stacked.reshape(2, groups, quarter, blocks_here, width)
    moved = lax.all_to_all(pieces, "tp", split_axis=1, concat_axis=3, tiled=True)
    placed = lax.all_to_all(moved, "fs", split_axis=3, concat_axis=2, tiled=True)
    own = placed.reshape(2, shards, quarter, width)
    right = lax.ppermute(own, "tp", ring(groups, 1))
    left = lax.ppermute(own, "tp", ring(groups, -1))
    far_up = lax.ppermute(right[0], "tp", ring(groups, 1))
    far_down = lax.ppermute(left[1], "tp", ring(groups, -1))
    values = tokens.astype(jnp.float32)
    scale = lax.rsqrt(jnp.mean(values * values, axis=1, keepdims=True) + epsilon)
    normed = (values * scale).astype(jnp.bfloat16)
    where = jnp.stack([lax.axis_index("tp"), lax.axis_index("fs") % CORES]).astype(jnp.int32)
    served = (shards, groups, quarter, width)
    packed_rows = rows_local * count // LANES
    vmem = pl.BlockSpec(memory_space=pltpu.VMEM)
    up_serving, down_serving, kept, away = pl.pallas_call(
        feed_forward,
        out_shape=[
            jax.ShapeDtypeStruct(served, jnp.bfloat16),
            jax.ShapeDtypeStruct(served, jnp.bfloat16),
            jax.ShapeDtypeStruct((chips, packed_rows, LANES), jnp.bfloat16),
            jax.ShapeDtypeStruct((chips, packed_rows, LANES), jnp.bfloat16),
        ],
        in_specs=[pl.BlockSpec(memory_space=pltpu.SMEM)] + [vmem] * 6,
        out_specs=[pl.BlockSpec(memory_space=pl.ANY)] * 2 + [vmem] * 2,
        scratch_shapes=[
            pltpu.VMEM(served, jnp.bfloat16),
            pltpu.VMEM(served, jnp.bfloat16),
            pltpu.SemaphoreType.DMA((2,)),
        ],
        compiler_params=pltpu.CompilerParams(vmem_limit_bytes=32 << 20),
        cost_estimate=pl.CostEstimate(
            flops=4 * count * features * width, bytes_accessed=4 * features * width * 2, transcendentals=0
        ),
        name="feed_forward",
    )(where, normed, own, left, right, far_up, far_down)
    other = lax.ppermute(away, "fs", [(i, i ^ 1) for i in range(shards)])
    summed = (kept.astype(jnp.float32) + other.astype(jnp.float32)).astype(jnp.bfloat16)
    same_core = [[z * CORES + c for z in range(chips)] for c in range(CORES)]
    arrived = lax.all_to_all(summed, "fs", 0, 0, axis_index_groups=same_core, tiled=True)
    out = unpacked(arrived.astype(jnp.float32).sum(axis=0), rows_local).T.astype(jnp.bfloat16)
    return (up_serving.reshape(features, width), down_serving.reshape(features, width), out)


def solution(mesh):
    in_specs = (P(("grp", "tp"), None), P("fs"), P("fs", "tp"), P("fs", "tp"))
    out_specs = (P("grp", "fs"), P("grp", "fs"), P(("grp", "tp"), "fs"))
    return jax.shard_map(local, mesh=mesh, in_specs=in_specs, out_specs=out_specs, check_vma=False)
```

time: 172 us -> 131 us (0.76)
  blocking collectives: 131 us -> 99.2 us
  waiting for transfers between devices: 26.4 us -> 18.2 us
  local copies, waits for them, and re-layouts: 4.06 us -> 0.82 us
  starting transfers between devices: 3.83 us -> 6.93 us
  matrix products: 2.28 us -> 0 us
  Pallas kernels: 0 us -> 2.17 us
    all_to_all x1, blocking collectives: 59.6 us -> 27.5 us  [local(): lax.all_to_all(summed, 'fs', 0, 0, axis_index_groups=same_core, tiled=True)]
    all_to_all x1 -> x0, waiting for transfers between devices: 26.4 us -> none  [copy_for_each(): lax.all_to_all(jnp.broadcast_to(x[None], (devices, *x.shape)), axis, 0, 0...]
    ppermute x0 -> x5, waiting for transfers between devices: none -> 18.2 us  [the longest x1 11.6 us: local(): right = lax.ppermute(own, 'tp', ring(groups, 1))]
    ppermute x0 -> x5, starting transfers between devices: none -> 6.93 us  [the longest x1 3.31 us: local(): far_down = lax.ppermute(left[1], 'tp', ring(groups, -1))]
    all_to_all x1 -> x0, starting transfers between devices: 3.83 us -> none  [copy_for_each(): lax.all_to_all(jnp.broadcast_to(x[None], (devices, *x.shape)), axis, 0, 0...]
    dot_general x1 -> x0, matrix products: 2.28 us -> none  [local(): lax.dot_general(down_serving, active, (((1,), (1,)), ((), ())), preferred...]
    pallas_call x0 -> x1, Pallas kernels: none -> 2.17 us  [local(): pl.pallas_call(feed_forward, out_shape=[jax.ShapeDtypeStruct(served, jnp....]
  transfers between devices with their start and end apart: 1 -> 5, of which waited for: 1 -> 3; matrix products, arithmetic and copies ran while one was open for 0% -> 0% of each run, Pallas kernels for 0% -> 0%
where the time goes in v2:
time: 131 us
  blocking collectives  99.2 us (76%)
  waiting for transfers between devices  18.2 us (14%)
  starting transfers between devices  6.93 us (5%)
  other arithmetic  2.59 us (2%)
  Pallas kernels  2.17 us (2%)
    all_to_all x1, blocking collectives, local(): lax.all_to_all(moved, 'fs', split_axis=3, concat_axis=2, tiled=True)  57.8 us
    all_to_all x1, blocking collectives, local(): lax.all_to_all(summed, 'fs', 0, 0, axis_index_groups=same_core, tiled=True)  27.5 us
    all_to_all x1, blocking collectives, local(): lax.all_to_all(pieces, 'tp', split_axis=1, concat_axis=3, tiled=True)  13.9 us
    ppermute x1, waiting for transfers between devices, local(): right = lax.ppermute(own, 'tp', ring(groups, 1))  11.6 us
    ppermute x1, waiting for transfers between devices, local(): far_up = lax.ppermute(right[0], 'tp', ring(groups, 1))  4.91 us
    ppermute x1, starting transfers between devices, local(): far_down = lax.ppermute(left[1], 'tp', ring(groups, -1))  3.31 us
    ppermute x1, starting transfers between devices, local(): left = lax.ppermute(own, 'tp', ring(groups, -1))  2.67 us
  transfers between devices with their start and end apart: 5, of which 3 were waited for; matrix products, arithmetic and copies ran while one was open for 0% of the time, Pallas kernels for 0%

profile of v2, /device:TPU:40, one launch (start us, length us, event | category | flops | bytes accessed | tf_op | source)
XLA Modules:
  0.0 130.7 jit_solution(16497697562292101992)
XLA Ops:
  0.6 1.2 multiply_convert_fusion
  1.8 0.1 copy.14
  2.1 0.1 copy.10
  2.2 13.9 %all_to_all.38 = bf16[2,4,16,8,256]{4,2,3,0,1:T(8,128)(2,1)S(1)} all-to-all(bf16[2,4,16,8,256]{4,2,3,0,1:T(8,128)(2,1)S(1)} %copy.10), channel_id=1, replica_groups=mesh['grp'=2,'fs'=32,'tp'=4] {'tp'}, dimensions={1} | all-to-all | bytes 1048576 | tf_op jit(solution)/shard_map/all_to_all | solution.py:74
  16.1 0.2 copy.19
  16.3 0.3 copy.12
  16.6 57.8 %all_to_all.39 = bf16[2,1,16,32,256]{4,2,0,1,3:T(8,128)(2,1)S(1)} all-to-all(bf16[2,1,16,32,256]{4,2,0,1,3:T(8,128)(2,1)S(1)} %copy.12), channel_id=1, replica_groups=mesh['grp'=2,'fs'=32,'tp'=4] {'fs'}, dimensions={3} | all-to-all | bytes 1048576 | tf_op jit(solution)/shard_map/all_to_all | solution.py:75
  74.4 0.7 collective-permute-start.1
  75.1 2.7 %collective-permute-start = (bf16[2,32,16,256]{3,2,1,0:T(8,128)(2,1)S(1)}, bf16[2,32,16,256]{3,2,1,0:T(8,128)(2,1)S(1)}, u32[]{:S(2)}, u32[]{:S(2)}) collective-permute-start(bf16[2,32,16,256]{3,2,1,0:T(8,128)(2,1)S(1)} %bitcast.31), channel_id=1, source_target_pairs={{0,3},{1,0},{2,1},{3,2},{4,7},{5,4},{6,5},{7,6},{8,11},{9,8},{10,9... | collective-permute-start | bytes 1572872 | tf_op jit(solution)/shard_map/ppermute | solution.py:78
  77.8 0.2 fusion
  78.0 11.6 %collective-permute-done.1.right = bf16[2,32,16,256]{3,2,1,0:T(8,128)(2,1)S(1)} collective-permute-done((bf16[2,32,16,256]{3,2,1,0:T(8,128)(2,1)S(1)}, bf16[2,32,16,256]{3,2,1,0:T(8,128)(2,1)S(1)}, u32[]{:S(2)}, u32[]{:S(2)}) %collective-permute-start.1) | collective-permute-done | bytes 524320 | tf_op jit(solution)/shard_map/ppermute | solution.py:77
  89.6 0.1 collective-permute-start.2
  89.8 3.3 %collective-permute-start.3 = (bf16[32,16,256]{2,1,0:T(8,128)(2,1)S(1)}, bf16[32,16,256]{2,1,0:T(8,128)(2,1)S(1)}, u32[]{:S(2)}, u32[]{:S(2)}) collective-permute-start(bf16[32,16,256]{2,1,0:T(8,128)(2,1)S(1)} %slice_bitcast_fusion), channel_id=1, source_target_pairs={{0,3},{1,0},{2,1},{3,2},{4,7},{5,4},{6,5},{7,6},{8,11},{9,8},{10,9... | collective-permute-start | bytes 786440 | tf_op jit(solution)/shard_map/ppermute | solution.py:80
  93.1 0.2 fusion.1.normed
  93.3 0.1 pad_add_fusion.where
  93.4 4.9 %collective-permute-done.2.far_up = bf16[32,16,256]{2,1,0:T(8,128)(2,1)S(1)} collective-permute-done((bf16[32,16,256]{2,1,0:T(8,128)(2,1)S(1)}, bf16[32,16,256]{2,1,0:T(8,128)(2,1)S(1)}, u32[]{:S(2)}, u32[]{:S(2)}) %collective-permute-start.2) | collective-permute-done | bytes 262176 | tf_op jit(solution)/shard_map/ppermute | solution.py:79
  98.3 2.2 %feed_forward.1 = (bf16[32,4,16,256]{3,2,1,0:T(8,128)(2,1)}, bf16[32,4,16,256]{3,2,1,0:T(8,128)(2,1)}, bf16[16,96,128]{2,1,0:T(8,128)(2,1)S(1)}, bf16[16,96,128]{2,1,0:T(8,128)(2,1)S(1)}) custom-call(s32[2]{0:T(128)S(1)} %pad_add_fusion.where, bf16[192,2048]{1,0:T(8,128)(2,1)S(1)} %fusion.1.normed, bf16[2,32,16,256]{3,2,1,0:T(8,128)(2,1)S(1)} %bitcast.32, ...), custom_call_target="tpu_custom_call" | custom-call | flops 402653184 | bytes 4194304 | tf_op jit(solution)/shard_map/feed_forward/pallas_call | solution.py:88
  100.4 0.1 collective-permute-start.4
  100.6 1.7 %collective-permute-done.4 = bf16[16,96,128]{2,1,0:T(8,128)(2,1)S(1)} collective-permute-done((bf16[16,96,128]{2,1,0:T(8,128)(2,1)S(1)}, bf16[16,96,128]{2,1,0:T(8,128)(2,1)S(1)}, u32[]{:S(2)}, u32[]{:S(2)}) %collective-permute-start.4) | collective-permute-done | bytes 393248 | tf_op jit(solution)/shard_map/ppermute | solution.py:109
  102.3 0.1 add_convert_fusion
  102.4 27.5 %all_to_all.40 = bf16[16,96,128]{2,1,0:T(8,128)(2,1)S(1)} all-to-all(bf16[16,96,128]{2,1,0:T(8,128)(2,1)S(1)} %add_convert_fusion), channel_id=1, replica_groups={{0,8,16,24,32,40,48,56,64,72,80,88,96,104,112,120},{4,12,20,28,36,44,52..., dimensions={0} | all-to-all | bytes 786432 | tf_op jit(solution)/shard_map/all_to_all | solution.py:112
  129.9 0.1 reduce
  130.0 0.1 fusion.2
  130.0 0.6 maximum_bitcast_fusion
  (14 shorter events, 0.2 us)
Async XLA Ops:
  0.6 1.3 copy-start.1
  16.6 61.2 %copy-start = (bf16[192,2048]{1,0:T(8,128)(2,1)S(1)}, bf16[192,2048]{1,0:T(8,128)(2,1)}, u32[]{:S(2)}) copy-start(bf16[192,2048]{1,0:T(8,128)(2,1)} %param.4) | copy-start | bytes 2359300
  74.4 15.2 %collective-permute-start.1 = (bf16[2,32,16,256]{3,2,1,0:T(8,128)(2,1)S(1)}, bf16[2,32,16,256]{3,2,1,0:T(8,128)(2,1)S(1)}, u32[]{:S(2)}, u32[]{:S(2)}) collective-permute-start(bf16[2,32,16,256]{3,2,1,0:T(8,128)(2,1)S(1)} %bitcast.30), channel_id=1, source_target_pairs={{0,1},{1,2},{2,3},{3,0},{4,5},{5,6},{6,7},{7,4},{8,9},{9,10},{10,1... | collective-permute-start | bytes 1572872 | tf_op jit(solution)/shard_map/ppermute | solution.py:77
  75.1 14.6 %collective-permute-start = (bf16[2,32,16,256]{3,2,1,0:T(8,128)(2,1)S(1)}, bf16[2,32,16,256]{3,2,1,0:T(8,128)(2,1)S(1)}, u32[]{:S(2)}, u32[]{:S(2)}) collective-permute-start(bf16[2,32,16,256]{3,2,1,0:T(8,128)(2,1)S(1)} %bitcast.31), channel_id=1, source_target_pairs={{0,3},{1,0},{2,1},{3,2},{4,7},{5,4},{6,5},{7,6},{8,11},{9,8},{10,9... | collective-permute-start | bytes 1572872 | tf_op jit(solution)/shard_map/ppermute | solution.py:78
  89.6 8.7 %collective-permute-start.2 = (bf16[32,16,256]{2,1,0:T(8,128)(2,1)S(1)}, bf16[32,16,256]{2,1,0:T(8,128)(2,1)S(1)}, u32[]{:S(2)}, u32[]{:S(2)}) collective-permute-start(bf16[32,16,256]{2,1,0:T(8,128)(2,1)S(1)} %slice_bitcast_fusion.1), channel_id=1, source_target_pairs={{0,1},{1,2},{2,3},{3,0},{4,5},{5,6},{6,7},{7,4},{8,9},{9,10},{10,1... | collective-permute-start | bytes 786440 | tf_op jit(solution)/shard_map/ppermute | solution.py:79
  89.8 8.5 %collective-permute-start.3 = (bf16[32,16,256]{2,1,0:T(8,128)(2,1)S(1)}, bf16[32,16,256]{2,1,0:T(8,128)(2,1)S(1)}, u32[]{:S(2)}, u32[]{:S(2)}) collective-permute-start(bf16[32,16,256]{2,1,0:T(8,128)(2,1)S(1)} %slice_bitcast_fusion), channel_id=1, source_target_pairs={{0,3},{1,0},{2,1},{3,2},{4,7},{5,4},{6,5},{7,6},{8,11},{9,8},{10,9... | collective-permute-start | bytes 786440 | tf_op jit(solution)/shard_map/ppermute | solution.py:80
  100.4 1.8 %collective-permute-start.4 = (bf16[16,96,128]{2,1,0:T(8,128)(2,1)S(1)}, bf16[16,96,128]{2,1,0:T(8,128)(2,1)S(1)}, u32[]{:S(2)}, u32[]{:S(2)}) collective-permute-start(bf16[16,96,128]{2,1,0:T(8,128)(2,1)S(1)} %get-tuple-element.10), channel_id=1, source_target_pairs={{0,4},{4,0},{8,12},{12,8},{16,20},{20,16},{24,28},{28,24},{32,36},... | collective-permute-start | bytes 1179656 | tf_op jit(solution)/shard_map/ppermute | solution.py:109

commit v3 on v2

--- a/solution.py
+++ b/solution.py
@@ -21,7 +21,7 @@
 
 
 def feed_forward(
-    where, normed, own, left, right, far_up, far_down, up_out, down_out, kept, away, up, down, sems
+    cores, where, normed, own, left, right, far_up, far_down, up_out, down_out, kept, away, up, down, sems
 ):
     shards, groups, quarter, width = up.shape
     at, core = where[0], where[1]
@@ -41,9 +41,9 @@
     head, tail = active[:LANES], active[LANES:]
     none = jnp.zeros_like(tail)
     upper, lower = jnp.concatenate([tail, none]), jnp.concatenate([none, tail])
-    rows, chips = groups * quarter, shards // CORES
+    rows, chips = groups * quarter, shards // cores
     for out, side in ((away, 1 - core), (kept, core)):
-        weights = down.reshape(chips, CORES, rows, width)[:, pl.ds(side, 1)][:, 0]
+        weights = down.reshape(chips, cores, rows, width)[:, pl.ds(side, 1)][:, 0]
         out[:, :rows] = nt_dot(weights.reshape(chips * rows, width), head).astype(out.dtype).reshape(chips, rows, LANES)
         both = nt_dot(weights[:, : rows // 2].reshape(chips * rows // 2, width), upper) + nt_dot(
             weights[:, rows // 2 :].reshape(chips * rows // 2, width), lower
@@ -60,20 +60,21 @@
 
 
 def local(tokens, norm_gain, up_trained, down_trained):
-    shards = lax.axis_size("fs")
-    groups = lax.axis_size("tp")
-    chips = shards // CORES
+    chips, cores, groups = lax.axis_size("z"), lax.axis_size("core"), lax.axis_size("tp")
+    shards = chips * cores
     rows_local, cols_local = up_trained.shape
     count, features = tokens.shape
+    width = cols_local * groups // shards
+    blocks = cols_local // (width * cores)
+    quarter = rows_local // groups
     folded = (norm_gain[:, None] * up_trained).astype(jnp.bfloat16)
     stacked = jnp.stack([folded, down_trained.astype(jnp.bfloat16)])
-    width = cols_local * groups // shards
-    blocks_here = cols_local // width
-    quarter = rows_local // groups
-    pieces = stacked.reshape(2, groups, quarter, blocks_here, width)
-    moved = lax.all_to_all(pieces, "tp", split_axis=1, concat_axis=3, tiled=True)
-    placed = lax.all_to_all(moved, "fs", split_axis=3, concat_axis=2, tiled=True)
-    own = placed.reshape(2, shards, quarter, width)
+    pieces = stacked.reshape(2, groups, quarter, blocks, cores, width).transpose(4, 1, 3, 0, 2, 5)
+    pieces = pieces.reshape(cores * groups, blocks, 2, quarter, width)
+    moved = lax.all_to_all(pieces, ("core", "tp"), 0, 0, tiled=True)
+    moved = moved.reshape(cores, chips, 2, quarter, width).transpose(1, 2, 0, 3, 4)
+    own = lax.all_to_all(moved, "z", 0, 0, tiled=True)
+    own = own.transpose(1, 0, 2, 3, 4).reshape(2, shards, quarter, width)
     right = lax.ppermute(own, "tp", ring(groups, 1))
     left = lax.ppermute(own, "tp", ring(groups, -1))
     far_up = lax.ppermute(right[0], "tp", ring(groups, 1))
@@ -81,12 +82,12 @@
     values = tokens.astype(jnp.float32)
     scale = lax.rsqrt(jnp.mean(values * values, axis=1, keepdims=True) + epsilon)
     normed = (values * scale).astype(jnp.bfloat16)
-    where = jnp.stack([lax.axis_index("tp"), lax.axis_index("fs") % CORES]).astype(jnp.int32)
+    where = jnp.stack([lax.axis_index("tp"), lax.axis_index("core")]).astype(jnp.int32)
     served = (shards, groups, quarter, width)
     packed_rows = rows_local * count // LANES
     vmem = pl.BlockSpec(memory_space=pltpu.VMEM)
     up_serving, down_serving, kept, away = pl.pallas_call(
-        feed_forward,
+        functools.partial(feed_forward, cores),
         out_shape=[
             jax.ShapeDtypeStruct(served, jnp.bfloat16),
             jax.ShapeDtypeStruct(served, jnp.bfloat16),
@@ -106,15 +107,18 @@
         ),
         name="feed_forward",
     )(where, normed, own, left, right, far_up, far_down)
-    other = lax.ppermute(away, "fs", [(i, i ^ 1) for i in range(shards)])
+    other = lax.ppermute(away, "core", ring(cores, 1))
     summed = (kept.astype(jnp.float32) + other.astype(jnp.float32)).astype(jnp.bfloat16)
-    same_core = [[z * CORES + c for z in range(chips)] for c in range(CORES)]
-    arrived = lax.all_to_all(summed, "fs", 0, 0, axis_index_groups=same_core, tiled=True)
+    arrived = lax.all_to_all(summed, "z", 0, 0, tiled=True)
     out = unpacked(arrived.astype(jnp.float32).sum(axis=0), rows_local).T.astype(jnp.bfloat16)
     return (up_serving.reshape(features, width), down_serving.reshape(features, width), out)
 
 
 def solution(mesh):
-    in_specs = (P(("grp", "tp"), None), P("fs"), P("fs", "tp"), P("fs", "tp"))
-    out_specs = (P("grp", "fs"), P("grp", "fs"), P(("grp", "tp"), "fs"))
+    sizes = mesh.shape
+    devices = mesh.devices.reshape(sizes["grp"], sizes["fs"] // CORES, CORES, sizes["tp"])
+    mesh = jax.sharding.Mesh(devices, ("grp", "z", "core", "tp"))
+    fs = ("z", "core")
+    in_specs = (P(("grp", "tp"), None), P(fs), P(fs, "tp"), P(fs, "tp"))
+    out_specs = (P("grp", fs), P("grp", fs), P(("grp", "tp"), fs))
     return jax.shard_map(local, mesh=mesh, in_specs=in_specs, out_specs=out_specs, check_vma=False)

time: 131 us -> 130 us (level)
  waiting for transfers between devices: 18.2 us -> 15.3 us
    ppermute x1, waiting for transfers between devices: 11.6 us -> 9.71 us  [local(): right = lax.ppermute(own, 'tp', ring(groups, 1))]
where the time goes in v3:
time: 130 us
  blocking collectives  100 us (77%)
  waiting for transfers between devices  15.3 us (12%)
  starting transfers between devices  6.93 us (5%)
  other arithmetic  3.28 us (3%)
  Pallas kernels  2.17 us (2%)
    all_to_all x1, blocking collectives, local(): own = lax.all_to_all(moved, 'z', 0, 0, tiled=True)  52.9 us
    all_to_all x1, blocking collectives, local(): arrived = lax.all_to_all(summed, 'z', 0, 0, tiled=True)  33.4 us
    all_to_all x1, blocking collectives, local(): moved = lax.all_to_all(pieces, ('core', 'tp'), 0, 0, tiled=True)  14.1 us
    ppermute x1, waiting for transfers between devices, local(): right = lax.ppermute(own, 'tp', ring(groups, 1))  9.71 us
    ppermute x1, waiting for transfers between devices, local(): far_up = lax.ppermute(right[0], 'tp', ring(groups, 1))  3.93 us
    ppermute x1, starting transfers between devices, local(): far_down = lax.ppermute(left[1], 'tp', ring(groups, -1))  3.31 us
  transfers between devices with their start and end apart: 5, of which 3 were waited for; matrix products, arithmetic and copies ran while one was open for 0% of the time, Pallas kernels for 0%

profile of v3, /device:TPU:40, one launch (start us, length us, event | category | flops | bytes accessed | tf_op | source)
XLA Modules:
  0.0 129.6 jit_solution(6052807965515611119)
XLA Ops:
  0.6 1.2 multiply_convert_fusion
  1.8 0.2 stack.21
  2.1 0.2 stack.22
  2.3 0.7 maximum_bitcast_fusion
  3.0 0.1 copy.10
  3.1 14.1 %all_to_all.15 = bf16[8,4,2,16,256]{4,3,2,1,0:T(8,128)(2,1)S(1)} all-to-all(bf16[8,4,2,16,256]{4,3,2,1,0:T(8,128)(2,1)S(1)} %bitcast.21), channel_id=1, replica_groups=mesh['grp'=2,'z'=16,'core'=2,'tp'=4] {'core','tp'}, dimensions={0} | all-to-all | bytes 1048576 | tf_op jit(solution)/shard_map/all_to_all | solution.py:74
  17.2 52.9 %all_to_all.16 = bf16[16,2,2,16,256]{4,3,1,2,0:T(8,128)(2,1)S(1)} all-to-all(bf16[16,2,2,16,256]{4,3,1,2,0:T(8,128)(2,1)S(1)} %copy.11), channel_id=1, replica_groups=mesh['grp'=2,'z'=16,'core'=2,'tp'=4] {'z'}, dimensions={0} | all-to-all | bytes 1048576 | tf_op jit(solution)/shard_map/all_to_all | solution.py:76
  70.2 1.0 collective-permute-start.1
  71.2 2.4 %collective-permute-start = (bf16[2,32,16,256]{3,2,1,0:T(8,128)(2,1)S(1)}, bf16[2,32,16,256]{3,2,1,0:T(8,128)(2,1)S(1)}, u32[]{:S(2)}, u32[]{:S(2)}) collective-permute-start(bf16[2,32,16,256]{3,2,1,0:T(8,128)(2,1)S(1)} %bitcast.19), channel_id=1, source_target_pairs={{0,3},{1,0},{2,1},{3,2},{4,7},{5,4},{6,5},{7,6},{8,11},{9,8},{10,9... | collective-permute-start | bytes 1572872 | tf_op jit(solution)/shard_map/ppermute | solution.py:79
  73.6 0.2 fusion
  73.8 9.7 %collective-permute-done.1.right = bf16[2,32,16,256]{3,2,1,0:T(8,128)(2,1)S(1)} collective-permute-done((bf16[2,32,16,256]{3,2,1,0:T(8,128)(2,1)S(1)}, bf16[2,32,16,256]{3,2,1,0:T(8,128)(2,1)S(1)}, u32[]{:S(2)}, u32[]{:S(2)}) %collective-permute-start.1) | collective-permute-done | bytes 524320 | tf_op jit(solution)/shard_map/ppermute | solution.py:78
  83.5 0.1 collective-permute-start.2
  83.7 3.3 %collective-permute-start.3 = (bf16[32,16,256]{2,1,0:T(8,128)(2,1)S(1)}, bf16[32,16,256]{2,1,0:T(8,128)(2,1)S(1)}, u32[]{:S(2)}, u32[]{:S(2)}) collective-permute-start(bf16[32,16,256]{2,1,0:T(8,128)(2,1)S(1)} %slice_bitcast_fusion), channel_id=1, source_target_pairs={{0,3},{1,0},{2,1},{3,2},{4,7},{5,4},{6,5},{7,6},{8,11},{9,8},{10,9... | collective-permute-start | bytes 786440 | tf_op jit(solution)/shard_map/ppermute | solution.py:81
  87.0 0.2 fusion.1.normed
  87.2 0.1 pad_add_fusion.where
  87.3 3.9 %collective-permute-done.2.far_up = bf16[32,16,256]{2,1,0:T(8,128)(2,1)S(1)} collective-permute-done((bf16[32,16,256]{2,1,0:T(8,128)(2,1)S(1)}, bf16[32,16,256]{2,1,0:T(8,128)(2,1)S(1)}, u32[]{:S(2)}, u32[]{:S(2)}) %collective-permute-start.2) | collective-permute-done | bytes 262176 | tf_op jit(solution)/shard_map/ppermute | solution.py:80
  91.2 2.2 %feed_forward.1 = (bf16[32,4,16,256]{3,2,1,0:T(8,128)(2,1)}, bf16[32,4,16,256]{3,2,1,0:T(8,128)(2,1)}, bf16[16,96,128]{2,1,0:T(8,128)(2,1)S(1)}, bf16[16,96,128]{2,1,0:T(8,128)(2,1)S(1)}) custom-call(s32[2]{0:T(128)S(1)} %pad_add_fusion.where, bf16[192,2048]{1,0:T(8,128)(2,1)S(1)} %fusion.1.normed, bf16[2,32,16,256]{3,2,1,0:T(8,128)(2,1)S(1)} %bitcast.20, ...), custom_call_target="tpu_custom_call" | custom-call | flops 402653184 | bytes 4194304 | tf_op jit(solution)/shard_map/feed_forward/pallas_call | solution.py:89
  93.4 0.1 collective-permute-start.4
  93.6 1.7 %collective-permute-done.4 = bf16[16,96,128]{2,1,0:T(8,128)(2,1)S(1)} collective-permute-done((bf16[16,96,128]{2,1,0:T(8,128)(2,1)S(1)}, bf16[16,96,128]{2,1,0:T(8,128)(2,1)S(1)}, u32[]{:S(2)}, u32[]{:S(2)}) %collective-permute-start.4) | collective-permute-done | bytes 393248 | tf_op jit(solution)/shard_map/ppermute | solution.py:110
  95.3 0.1 add_convert_fusion
  95.4 33.4 %all_to_all.17 = bf16[16,96,128]{2,1,0:T(8,128)(2,1)S(1)} all-to-all(bf16[16,96,128]{2,1,0:T(8,128)(2,1)S(1)} %add_convert_fusion), channel_id=1, replica_groups=mesh['grp'=2,'z'=16,'core'=2,'tp'=4] {'z'}, dimensions={0} | all-to-all | bytes 786432 | tf_op jit(solution)/shard_map/all_to_all | solution.py:112
  128.8 0.1 reduce
  128.9 0.1 fusion.2
  129.0 0.6 maximum_bitcast_fusion.1
  (13 shorter events, 0.2 us)
Async XLA Ops:
  0.6 1.4 %copy-start.1 = (f32[64,2048]{1,0:T(8,128)S(1)}, f32[64,2048]{1,0:T(8,128)}, u32[]{:S(2)}) copy-start(f32[64,2048]{1,0:T(8,128)} %param.7) | copy-start | bytes 1572868
  17.2 56.3 %copy-start = (bf16[192,2048]{1,0:T(8,128)(2,1)S(1)}, bf16[192,2048]{1,0:T(8,128)(2,1)}, u32[]{:S(2)}) copy-start(bf16[192,2048]{1,0:T(8,128)(2,1)} %param.4) | copy-start | bytes 2359300
  70.2 13.3 %collective-permute-start.1 = (bf16[2,32,16,256]{3,2,1,0:T(8,128)(2,1)S(1)}, bf16[2,32,16,256]{3,2,1,0:T(8,128)(2,1)S(1)}, u32[]{:S(2)}, u32[]{:S(2)}) collective-permute-start(bf16[2,32,16,256]{3,2,1,0:T(8,128)(2,1)S(1)} %bitcast.18), channel_id=1, source_target_pairs={{0,1},{1,2},{2,3},{3,0},{4,5},{5,6},{6,7},{7,4},{8,9},{9,10},{10,1... | collective-permute-start | bytes 1572872 | tf_op jit(solution)/shard_map/ppermute | solution.py:78
  71.2 12.5 %collective-permute-start = (bf16[2,32,16,256]{3,2,1,0:T(8,128)(2,1)S(1)}, bf16[2,32,16,256]{3,2,1,0:T(8,128)(2,1)S(1)}, u32[]{:S(2)}, u32[]{:S(2)}) collective-permute-start(bf16[2,32,16,256]{3,2,1,0:T(8,128)(2,1)S(1)} %bitcast.19), channel_id=1, source_target_pairs={{0,3},{1,0},{2,1},{3,2},{4,7},{5,4},{6,5},{7,6},{8,11},{9,8},{10,9... | collective-permute-start | bytes 1572872 | tf_op jit(solution)/shard_map/ppermute | solution.py:79
  83.5 7.7 %collective-permute-start.2 = (bf16[32,16,256]{2,1,0:T(8,128)(2,1)S(1)}, bf16[32,16,256]{2,1,0:T(8,128)(2,1)S(1)}, u32[]{:S(2)}, u32[]{:S(2)}) collective-permute-start(bf16[32,16,256]{2,1,0:T(8,128)(2,1)S(1)} %slice_bitcast_fusion.1), channel_id=1, source_target_pairs={{0,1},{1,2},{2,3},{3,0},{4,5},{5,6},{6,7},{7,4},{8,9},{9,10},{10,1... | collective-permute-start | bytes 786440 | tf_op jit(solution)/shard_map/ppermute | solution.py:80
  83.7 7.5 %collective-permute-start.3 = (bf16[32,16,256]{2,1,0:T(8,128)(2,1)S(1)}, bf16[32,16,256]{2,1,0:T(8,128)(2,1)S(1)}, u32[]{:S(2)}, u32[]{:S(2)}) collective-permute-start(bf16[32,16,256]{2,1,0:T(8,128)(2,1)S(1)} %slice_bitcast_fusion), channel_id=1, source_target_pairs={{0,3},{1,0},{2,1},{3,2},{4,7},{5,4},{6,5},{7,6},{8,11},{9,8},{10,9... | collective-permute-start | bytes 786440 | tf_op jit(solution)/shard_map/ppermute | solution.py:81
  93.4 1.8 %collective-permute-start.4 = (bf16[16,96,128]{2,1,0:T(8,128)(2,1)S(1)}, bf16[16,96,128]{2,1,0:T(8,128)(2,1)S(1)}, u32[]{:S(2)}, u32[]{:S(2)}) collective-permute-start(bf16[16,96,128]{2,1,0:T(8,128)(2,1)S(1)} %get-tuple-element.10), channel_id=1, source_target_pairs={{0,4},{4,0},{1,5},{5,1},{2,6},{6,2},{3,7},{7,3},{8,12},{12,8},{9,1... | collective-permute-start | bytes 1179656 | tf_op jit(solution)/shard_map/ppermute | solution.py:110
